TPU v7x, 32 devices: a whole 2x2x4 slice. The times are simulated.
32 devices in a mesh: sp: 8 (over z, y), tp: 4 (over x, core).
Axes of the slice: x: 2, y: 2, z: 4, core: 2. Of those that a mesh axis runs over, the one named last changes fastest.
Arguments:
- queries: bfloat16 [3072, 2048], P('sp', 'tp'), may hold values from -200 to 200
- keys: bfloat16 [3072, 2048], P('sp', 'tp'), may hold values from -200 to 200
- values: bfloat16 [3072, 2048], P('sp', 'tp'), may hold values from -6 to 6
- forget_sums: float32 [3072, 16], P('sp', 'tp'), may hold values from -3072 to 0, as said below
- residual_in: bfloat16 [3072, 2048], P(('sp', 'tp')), may hold values from -0.59765625 to 0.59765625
- out_weight: bfloat16 [2048, 2048], P('tp'), may hold values from -0.125 to 0.125
- norm_gain: bfloat16 [2048], replicated, may hold values from 0.099609375 to 1.8984375
- gate_weight: bfloat16 [2048, 3072], P('sp', 'tp'), may hold values from -0.125 to 0.125
- up_weight: bfloat16 [2048, 3072], P('sp', 'tp'), may hold values from -0.125 to 0.125
- down_weight: bfloat16 [3072, 2048], P('tp', 'sp'), may hold values from -0.109375 to 0.109375
Outputs:
- mixed: bfloat16 [3072, 2048], P(('sp', 'tp'))
Inputs may be any that keep to these rules, and one draw needn't show every extreme that they name: `forget_sums`: in every head the entries never rise from one position to the next.
All inputs are finite; a program needn't handle non-finite values.
Results may differ from a plain program's by a relative error of at most 0.022.
Values may be sent and summed in bfloat16 or wider, within the bound.
A program may use at most 192 MiB of HBM per device.

v0:
```python
import math
import jax
import jax.numpy as jnp
from jax import lax
from jax.sharding import PartitionSpec as P

HD = 128


def attend_block(carried, block, query_rows, query_gate, query_pos, heads_here):
    row_top, row_total, weighted = carried
    key_rows, value_rows, key_gate, key_pos = block
    score_scale = HD ** (-0.5)
    tops, totals, sums = ([], [], [])
    for head_index in range(heads_here):
        columns = slice(head_index * HD, (head_index + 1) * HD)
        scores = (
            jnp.einsum(
                "qd,kd->qk",
                query_rows[:, columns],
                key_rows[:, columns],
                preferred_element_type=jnp.float32,
            )
            * score_scale
        )
        scores = scores + query_gate[:, head_index : head_index + 1] - key_gate[None, :, head_index]
        scores = jnp.where(key_pos[None, :] <= query_pos[:, None], scores, -jnp.inf)
        new_top = jnp.maximum(row_top[:, head_index], jnp.max(scores, axis=1))
        shrink = jnp.exp(row_top[:, head_index] - new_top)
        expon = jnp.exp(scores - new_top[:, None])
        totals.append(shrink * row_total[:, head_index] + jnp.sum(expon, axis=1))
        sums.append(
            shrink[:, None] * weighted[:, columns]
            + jnp.dot(
                expon.astype(jnp.bfloat16),
                value_rows[:, columns],
                preferred_element_type=jnp.float32,
            )
        )
        tops.append(new_top)
    return (jnp.stack(tops, axis=1), jnp.stack(totals, axis=1), jnp.concatenate(sums, axis=1))


def shards(
    queries,
    keys,
    values,
    forget_sums,
    residual_in,
    out_weight,
    norm_gain,
    gate_weight,
    up_weight,
    down_weight,
):
    rows_here = queries.shape[0]
    heads_here = queries.shape[1] // HD
    first = lax.axis_index("sp") * rows_here
    query_pos = first + jnp.arange(rows_here, dtype=jnp.int32)
    early_gate, early_up = (
        lax.all_gather(gate_weight, "sp", axis=0, tiled=True),
        lax.all_gather(up_weight, "sp", axis=0, tiled=True),
    )
    all_gates = lax.all_gather(forget_sums, "sp", axis=0, tiled=True)
    start_state = (
        jnp.full((rows_here, heads_here), -1e30, jnp.float32),
        jnp.zeros((rows_here, heads_here), jnp.float32),
        jnp.zeros((rows_here, heads_here * HD), jnp.float32),
    )
    carried = start_state
    key_rows = lax.all_gather(keys, "sp", axis=0, tiled=True)
    value_rows = lax.all_gather(values, "sp", axis=0, tiled=True)
    count = key_rows.shape[0]
    block_rows = math.gcd(count, 512)
    block_count = count // block_rows
    key_pos = jnp.arange(count, dtype=jnp.int32)
    blocks = (
        key_rows.reshape(block_count, block_rows, -1),
        value_rows.reshape(block_count, block_rows, -1),
        all_gates.reshape(block_count, block_rows, -1),
        key_pos.reshape(block_count, block_rows),
    )

    def advance(inner, block):
        return (attend_block(inner, block, queries, forget_sums, query_pos, heads_here), None)

    carried, unused = lax.scan(advance, carried, blocks)
    row_top, row_total, weighted = carried
    attended = (weighted / jnp.repeat(row_total, HD, axis=1)).astype(jnp.bfloat16)
    projected = lax.psum_scatter(
        jnp.dot(attended, out_weight, preferred_element_type=jnp.float32).astype(jnp.bfloat16),
        "tp",
        scatter_dimension=0,
        tiled=True,
    ).astype(jnp.float32)
    stream = residual_in.astype(jnp.float32) + projected
    normed = stream * lax.rsqrt(jnp.mean(stream * stream, axis=1, keepdims=True) + 1e-06)
    normed = (normed * norm_gain.astype(jnp.float32)).astype(jnp.bfloat16)
    every_row = lax.all_gather(normed, "tp", axis=0, tiled=True)
    gate = jnp.dot(every_row, early_gate, preferred_element_type=jnp.float32)
    up = jnp.dot(every_row, early_up, preferred_element_type=jnp.float32)
    hidden = (jax.nn.silu(gate) * up).astype(jnp.bfloat16)
    partial_value = jnp.dot(
        hidden,
        lax.all_gather(down_weight, "sp", axis=1, tiled=True),
        preferred_element_type=jnp.float32,
    ).astype(jnp.bfloat16)
    summed = lax.psum_scatter(
        partial_value.astype(jnp.float32).astype(jnp.bfloat16),
        "tp",
        scatter_dimension=0,
        tiled=True,
    ).astype(jnp.float32)
    return (stream + summed).astype(jnp.bfloat16)


def solution(mesh):
    placed = (
        P("sp", "tp"),
        P("sp", "tp"),
        P("sp", "tp"),
        P("sp", "tp"),
        P(("sp", "tp"), None),
        P("tp", None),
        P(),
        P("sp", "tp"),
        P("sp", "tp"),
        P("tp", "sp"),
    )
    return jax.shard_map(
        shards, mesh=mesh, in_specs=placed, out_specs=P(("sp", "tp"), None), check_vma=False
    )
```

profile of v0, /device:TPU:0, one launch (start us, length us, event | category | flops | bytes accessed | tf_op | source)
XLA Modules:
  0.0 441.7 jit_solution(3732854181924096891)
XLA Ops:
  6.5 0.7 all-gather.7.cloned.1.call-update
  7.3 0.7 all-gather.9.cloned.1.call-update
  8.1 32.9 %all_gather.22 = f32[3072,4]{0,1:T(4,128)S(1)} all-gather(f32[384,4]{0,1:T(4,128)} %param.15), channel_id=1, replica_groups=mesh['sp'=8,'tp'=4] {'sp'}, dimensions={0}, use_global_device_ids=true | all-gather | bytes 55296 | tf_op jit(solution)/shard_map/all_gather | solution.py:64
  41.0 31.5 %all-gather.7.cloned.1.call-done = bf16[3072,512]{1,0:T(8,128)(2,1)} async-done(((bf16[384,512]{1,0:T(8,128)(2,1)}), bf16[3072,512]{1,0:T(8,128)(2,1)}) %all-gather.7.cloned.1.call-update) | async-done | bytes 3145744 | tf_op jit(solution)/shard_map/all_gather | solution.py:71
  72.5 60.9 %all-gather.9.cloned.1.call-done = bf16[3072,512]{1,0:T(8,128)(2,1)} async-done(((bf16[384,512]{1,0:T(8,128)(2,1)}), bf16[3072,512]{1,0:T(8,128)(2,1)}) %all-gather.9.cloned.1.call-update) | async-done | bytes 3145744 | tf_op jit(solution)/shard_map/all_gather | solution.py:72
  133.5 28.8 %while.15 = (s32[]{:T(128)}, f32[384,4]{0,1:T(4,128)S(1)}, f32[384,4]{0,1:T(4,128)S(1)}, f32[384,512]{0,1:T(8,128)S(1)}, s32[6,512]{1,0:T(8,128)S(1)}, /*index=5...) while((s32[]{:T(128)}, f32[384,4]{0,1:T(4,128)S(1)}, ...), condition=%wide.region_9.10_spmd.clone, body=%wide.region_0.9_spmd.clone.sunk | while | flops 411514752 | bytes 16326277 | solution.py:87
  133.5 1.3 dynamic-slice_bitcast_fusion.6
  134.9 0.3 fusion.90
  135.2 0.3 fusion.91
  135.6 0.4 fusion.92
  135.9 0.3 fusion.93
  138.3 1.3 dynamic-slice_bitcast_fusion.6
  139.7 0.3 fusion.90
  140.0 0.3 fusion.91
  140.4 0.3 fusion.92
  140.7 0.3 fusion.93
  143.1 1.3 dynamic-slice_bitcast_fusion.6
  144.5 0.3 fusion.90
  144.8 0.3 fusion.91
  145.2 0.3 fusion.92
  145.5 0.3 fusion.93
  147.9 1.3 dynamic-slice_bitcast_fusion.6
  149.3 0.3 fusion.90
  149.6 0.3 fusion.91
  150.0 0.3 fusion.92
  150.3 0.3 fusion.93
  152.7 1.3 dynamic-slice_bitcast_fusion.6
  154.1 0.3 fusion.90
  154.4 0.3 fusion.91
  154.8 0.3 fusion.92
  157.5 1.3 dynamic-slice_bitcast_fusion.6
  158.9 0.3 fusion.90
  159.6 0.3 fusion.92
  162.4 2.2 convolution_convert_fusion.1
  164.6 0.5 all-gather.13.cloned.1.call-update
  165.2 26.2 %reduce-scatter.3.cloned.1.call-done = bf16[96,2048]{1,0:T(8,128)(2,1)} async-done(((bf16[384,2048]{1,0:T(8,128)(2,1)}), bf16[96,2048]{1,0:T(8,128)(2,1)}) %reduce-scatter.3.cloned.1.call-update) | async-done | bytes 393232 | tf_op jit(solution)/shard_map/reduce_scatter | solution.py:90
  191.4 1.2 multiply_reduce_fusion
  192.7 1.9 multiply_convert_fusion
  194.7 0.5 all-gather.15.cloned.1.call-update
  195.2 0.7 all-gather.17.cloned.1.call-update
  196.0 57.5 %all-gather.13.cloned.1.call-done = bf16[2048,768]{1,0:T(8,128)(2,1)} async-done(((bf16[256,768]{1,0:T(8,128)(2,1)}), bf16[2048,768]{1,0:T(8,128)(2,1)}) %all-gather.13.cloned.1.call-update) | async-done | bytes 3145744 | tf_op jit(solution)/shard_map/all_gather | solution.py:61
  253.5 19.7 %all-gather.11.cloned.1.call-done = bf16[384,2048]{1,0:T(8,128)(2,1)} async-done(((bf16[96,2048]{1,0:T(8,128)(2,1)}), bf16[384,2048]{1,0:T(8,128)(2,1)}) %all-gather.11.cloned.1.call-update) | async-done | bytes 1572880 | tf_op jit(solution)/shard_map/all_gather | solution.py:99
  273.3 4.8 %fusion.55 = f32[384,768]{1,0:T(8,128)} fusion(bf16[384,2048]{1,0:T(8,128)(2,1)} %all-gather.11.cloned.1.call-done, bf16[2048,768]{1,0:T(8,128)(2,1)} %all-gather.13.cloned.1.call-done), kind=kOutput, calls=%fused_computation.100 | convolution fusion | flops 1207959552 | bytes 5898240 | tf_op jit(solution)/shard_map/dot_general | solution.py:100
  278.0 57.3 %all-gather.15.cloned.1.call-done = bf16[2048,768]{1,0:T(8,128)(2,1)} async-done(((bf16[256,768]{1,0:T(8,128)(2,1)}), bf16[2048,768]{1,0:T(8,128)(2,1)}) %all-gather.15.cloned.1.call-update) | async-done | bytes 3145744 | tf_op jit(solution)/shard_map/all_gather | solution.py:62
  335.4 63.4 %all-gather.17.cloned.1.call-done = bf16[768,2048]{1,0:T(8,128)(2,1)} async-done(((bf16[768,256]{1,0:T(8,128)(2,1)}), bf16[768,2048]{1,0:T(8,128)(2,1)}) %all-gather.17.cloned.1.call-update) | async-done | bytes 3145744 | tf_op jit(solution)/shard_map/all_gather | solution.py:105
  398.7 7.9 %convolution_convert_fusion = bf16[384,2048]{1,0:T(8,128)(2,1)} fusion(bf16[768,2048]{1,0:T(8,128)(2,1)} %all-gather.17.cloned.1.call-done, bf16[384,2048]{1,0:T(8,128)(2,1)} %all-gather.11.cloned.1.call-done, bf16[2048,768]{1,0:T(8,128)(2,1)} %all-gather.15.cloned.1.call-done, f32[384,768]{1,0:T(8,128)} %fusion.55), kind=kOutput, calls=%fused_computation.81 | convolution fusion | flops 2418475008 | bytes 10616832 | tf_op jit(solution)/shard_map/dot_general | solution.py:103
  406.6 26.4 %reduce-scatter.5.cloned.1.call-done = bf16[96,2048]{1,0:T(8,128)(2,1)} async-done(((bf16[384,2048]{1,0:T(8,128)(2,1)}), bf16[96,2048]{1,0:T(8,128)(2,1)}) %reduce-scatter.5.cloned.1.call-update) | async-done | bytes 393232 | tf_op jit(solution)/shard_map/reduce_scatter | solution.py:108
  433.0 1.9 add_convert_fusion
  (141 shorter events, 13.7 us)
Async XLA Ops:
  6.5 155.8 %copy-start = (bf16[512,2048]{1,0:T(8,128)(2,1)S(1)}, bf16[512,2048]{1,0:T(8,128)(2,1)}, u32[]{:S(2)}) copy-start(bf16[512,2048]{1,0:T(8,128)(2,1)} %param.17) | copy-start | bytes 6291460
  6.5 126.9 %copy-start.3 = (f32[384,4]{0,1:T(4,128)S(1)}, f32[384,4]{0,1:T(4,128)}, u32[]{:S(2)}) copy-start(f32[384,4]{0,1:T(4,128)} %param.15) | copy-start | bytes 18436
  6.5 126.9 %copy-start.5 = (bf16[384,512]{1,0:T(8,128)(2,1)S(1)}, bf16[384,512]{1,0:T(8,128)(2,1)}, u32[]{:S(2)}) copy-start(bf16[384,512]{1,0:T(8,128)(2,1)} %param.12) | copy-start | bytes 1179652
  6.5 65.9 %all-gather.7.cloned.1.call-start = ((), (), s32[]{:S(2)}) async-start(), calls=%async_computation.2 | async-start | bytes 3538944 | tf_op jit(solution)/shard_map/all_gather | solution.py:71
  7.3 126.1 %all-gather.9.cloned.1.call-start = ((), (), s32[]{:S(2)}) async-start(), calls=%async_computation.3 | async-start | bytes 3538944 | tf_op jit(solution)/shard_map/all_gather | solution.py:72
  8.0 183.4 %reduce-scatter.3.cloned.1.call-start = ((), (), s32[]{:S(2)}) async-start(), calls=%async_computation.4 | async-start | bytes 1966080 | tf_op jit(solution)/shard_map/reduce_scatter | solution.py:90
  164.5 0.7 copy-start.4
  164.5 26.9 %copy-start.1 = (bf16[96,2048]{1,0:T(8,128)(2,1)S(1)}, bf16[96,2048]{1,0:T(8,128)(2,1)}, u32[]{:S(2)}) copy-start(bf16[96,2048]{1,0:T(8,128)(2,1)} %param.16) | copy-start | bytes 1179652
  164.6 89.0 %all-gather.13.cloned.1.call-start = ((), (), s32[]{:S(2)}) async-start(), calls=%async_computation.6 | async-start | bytes 3538944 | tf_op jit(solution)/shard_map/all_gather | solution.py:61
  165.1 108.1 %all-gather.11.cloned.1.call-start = ((), (), s32[]{:S(2)}) async-start(), calls=%async_computation.5 | async-start | bytes 1966080 | tf_op jit(solution)/shard_map/all_gather | solution.py:99
  194.6 140.7 %all-gather.15.cloned.1.call-start = ((), (), s32[]{:S(2)}) async-start(), calls=%async_computation.7 | async-start | bytes 3538944 | tf_op jit(solution)/shard_map/all_gather | solution.py:62
  195.2 203.6 %all-gather.17.cloned.1.call-start = ((), (), s32[]{:S(2)}) async-start(), calls=%async_computation.8 | async-start | bytes 3538944 | tf_op jit(solution)/shard_map/all_gather | solution.py:105
  195.9 237.1 %reduce-scatter.5.cloned.1.call-start = ((), (), s32[]{:S(2)}) async-start(), calls=%async_computation.9 | async-start | bytes 1966080 | tf_op jit(solution)/shard_map/reduce_scatter | solution.py:108
  406.6 26.4 %copy-start.2 = (bf16[96,2048]{1,0:T(8,128)(2,1)S(1)}, bf16[96,2048]{1,0:T(8,128)(2,1)}, u32[]{:S(2)}) copy-start(bf16[96,2048]{1,0:T(8,128)(2,1)} %reduce-scatter.3.cloned.1.call-done) | copy-start | bytes 1179652
Sparse Core Ops, SparseCore 0:
  9.5 62.9 all-gather.6
  74.7 58.6 all-gather.8
  164.7 26.6 reduce-scatter.2
  193.5 60.0 all-gather.12
  254.9 18.2 all-gather.10
  275.3 60.0 all-gather.14
  337.4 61.2 all-gather.16
  406.7 26.2 reduce-scatter.4
where the time goes:
time: 442 us
  waiting for transfers between devices  346 us (78%)
  blocking collectives  32.9 us (7%)
  matrix products  30.1 us (7%)
  between operations  13.6 us (3%)
  other arithmetic  9.88 us (2%)
  local copies, waits for them, and re-layouts  8.11 us (2%)
    all_gather x1, waiting for transfers between devices, shards(): lax.all_gather(down_weight, 'sp', axis=1, tiled=True)  63.4 us
    all_gather x1, waiting for transfers between devices, shards(): value_rows = lax.all_gather(values, 'sp', axis=0, tiled=True)  60.9 us
    all_gather x1, waiting for transfers between devices, shards(): lax.all_gather(gate_weight, 'sp', axis=0, tiled=True)  57.5 us
    all_gather x1, waiting for transfers between devices, shards(): lax.all_gather(up_weight, 'sp', axis=0, tiled=True)  57.3 us
    all_gather x1, blocking collectives, shards(): all_gates = lax.all_gather(forget_sums, 'sp', axis=0, tiled=True)  32.9 us
    all_gather x1, waiting for transfers between devices, shards(): key_rows = lax.all_gather(keys, 'sp', axis=0, tiled=True)  31.5 us
    reduce_scatter x1, waiting for transfers between devices, shards(): lax.psum_scatter(partial_value.astype(jnp.float32).astype(jnp.bfloat16),...  26.4 us
    reduce_scatter x1, waiting for transfers between devices, shards(): lax.psum_scatter(jnp.dot(attended, out_weight, preferred_element_type=jnp...  26.2 us
  transfers between devices with their start and end apart: 8, of which 8 were waited for; matrix products, arithmetic and copies ran while one was open for 2% of the time, Pallas kernels for 0%

commit v1 on v0

--- a/solution.py
+++ b/solution.py
@@ -3,6 +3,7 @@
 import jax.numpy as jnp
 from jax import lax
 from jax.sharding import PartitionSpec as P
+from jax.lax import all_gather
 
 HD = 128
 
@@ -61,14 +62,19 @@
         lax.all_gather(gate_weight, "sp", axis=0, tiled=True),
         lax.all_gather(up_weight, "sp", axis=0, tiled=True),
     )
-    all_gates = lax.all_gather(forget_sums, "sp", axis=0, tiled=True)
     start_state = (
         jnp.full((rows_here, heads_here), -1e30, jnp.float32),
         jnp.zeros((rows_here, heads_here), jnp.float32),
         jnp.zeros((rows_here, heads_here * HD), jnp.float32),
     )
     carried = start_state
-    key_rows = lax.all_gather(keys, "sp", axis=0, tiled=True)
+    all_gates, key_rows = jnp.split(
+        all_gather(
+            jnp.concatenate([forget_sums, keys], axis=1), axis_name="sp", axis=0, tiled=True
+        ),
+        [forget_sums.shape[1]],
+        axis=1,
+    )
     value_rows = lax.all_gather(values, "sp", axis=0, tiled=True)
     count = key_rows.shape[0]
     block_rows = math.gcd(count, 512)

time: 442 us -> 500 us (1.13)
  waiting for transfers between devices: 346 us -> 423 us
  blocking collectives: 32.9 us -> 0 us
  local copies, waits for them, and re-layouts: 8.11 us -> 19.8 us
    all_gather x1, waiting for transfers between devices: 31.5 us -> 120 us  [shards(): all_gather(jnp.concatenate([forget_sums, keys], axis=1), axis_name='sp',...]
    all_gather x1 -> x0, blocking collectives: 32.9 us -> none  [shards(): all_gates = lax.all_gather(forget_sums, 'sp', axis=0, tiled=True)]
    all_gather x1, waiting for transfers between devices: 60.9 us -> 49.6 us  [shards(): value_rows = lax.all_gather(values, 'sp', axis=0, tiled=True)]
    split x0 -> x2, local copies, waits for them, and re-layouts: none -> 8.92 us  [shards(): jnp.split(all_gather(jnp.concatenate([forget_sums, keys], axis=1), axis_n...]
  transfers between devices with their start and end apart: 8 -> 8, of which waited for: 8 -> 8; matrix products, arithmetic and copies ran while one was open for 2% -> 4% of each run, Pallas kernels for 0% -> 0%
where the time goes in v1:
time: 500 us; the launch traced here: 499 us
  waiting for transfers between devices  423 us (85%)
  matrix products  30.1 us (6%)
  local copies, waits for them, and re-layouts  19.8 us (4%)
  between operations  13.6 us (3%)
  other arithmetic  12.4 us (2%)
    all_gather x1, waiting for transfers between devices, shards(): all_gather(jnp.concatenate([forget_sums, keys], axis=1), axis_name='sp',...  120 us
    all_gather x1, waiting for transfers between devices, shards(): lax.all_gather(down_weight, 'sp', axis=1, tiled=True)  63.4 us
    all_gather x1, waiting for transfers between devices, shards(): lax.all_gather(gate_weight, 'sp', axis=0, tiled=True)  57.6 us
    all_gather x1, waiting for transfers between devices, shards(): lax.all_gather(up_weight, 'sp', axis=0, tiled=True)  57.3 us
    all_gather x1, waiting for transfers between devices, shards(): value_rows = lax.all_gather(values, 'sp', axis=0, tiled=True)  49.6 us
    reduce_scatter x1, waiting for transfers between devices, shards(): lax.psum_scatter(partial_value.astype(jnp.float32).astype(jnp.bfloat16),...  26.4 us
    reduce_scatter x1, waiting for transfers between devices, shards(): lax.psum_scatter(jnp.dot(attended, out_weight, preferred_element_type=jnp...  26.1 us
    all_gather x1, waiting for transfers between devices, shards(): every_row = lax.all_gather(normed, 'tp', axis=0, tiled=True)  19.7 us
  transfers between devices with their start and end apart: 8, of which 8 were waited for; matrix products, arithmetic and copies ran while one was open for 4% of the time, Pallas kernels for 0%

profile of v1, /device:TPU:0, one launch (start us, length us, event | category | flops | bytes accessed | tf_op | source)
XLA Modules:
  0.0 499.4 jit_solution(13620481617680688380)
XLA Ops:
  6.5 1.2 convert_element_type.48
  7.8 0.8 copy.12
  8.6 1.3 pad_maximum_fusion.3
  10.0 0.7 all-gather.9.cloned.1.call-update
  10.7 120.0 %all-gather.7.cloned.1.call-done = f32[3072,516]{1,0:T(8,128)} async-done(((f32[384,516]{1,0:T(8,128)}), f32[3072,516]{1,0:T(8,128)}) %all-gather.7.cloned.1.call-update) | async-done | bytes 6340624 | tf_op jit(solution)/shard_map/all_gather | solution.py:72
  130.7 2.6 split.9
  133.4 1.9 copy.14
  135.3 6.3 %split.8 = bf16[3072,512]{1,0:T(8,128)(2,1)} slice(f32[3072,516]{1,0:T(8,128)} %all-gather.7.cloned.1.call-done), slice={[0:3072], [4:516]} | slice | bytes 6291456 | tf_op jit(solution)/shard_map/split | solution.py:71
  141.5 49.6 %all-gather.9.cloned.1.call-done = bf16[3072,512]{1,0:T(8,128)(2,1)} async-done(((bf16[384,512]{1,0:T(8,128)(2,1)}), bf16[3072,512]{1,0:T(8,128)(2,1)}) %all-gather.9.cloned.1.call-update) | async-done | bytes 3145744 | tf_op jit(solution)/shard_map/all_gather | solution.py:78
  191.2 28.8 %while.15 = (s32[]{:T(128)}, f32[384,4]{0,1:T(4,128)S(1)}, f32[384,4]{0,1:T(4,128)S(1)}, f32[384,512]{0,1:T(8,128)S(1)}, s32[6,512]{1,0:T(8,128)S(1)}, /*index=5...) while((s32[]{:T(128)}, f32[384,4]{0,1:T(4,128)S(1)}, ...), condition=%wide.region_9.10_spmd.clone, body=%wide.region_0.9_spmd.clone.sunk | while | flops 411514752 | bytes 16326277 | solution.py:93
  191.2 1.3 dynamic-slice_bitcast_fusion.6
  192.6 0.3 fusion.90
  193.0 0.3 fusion.91
  193.3 0.3 fusion.92
  193.7 0.3 fusion.93
  196.0 1.3 dynamic-slice_bitcast_fusion.6
  197.4 0.3 fusion.90
  197.8 0.3 fusion.91
  198.1 0.3 fusion.92
  198.5 0.3 fusion.93
  200.9 1.3 dynamic-slice_bitcast_fusion.6
  202.2 0.3 fusion.90
  202.6 0.3 fusion.91
  202.9 0.3 fusion.92
  205.7 1.3 dynamic-slice_bitcast_fusion.6
  207.0 0.3 fusion.90
  207.7 0.3 fusion.92
  210.5 1.3 dynamic-slice_bitcast_fusion.6
  211.8 0.3 fusion.90
  212.5 0.3 fusion.92
  215.3 1.3 dynamic-slice_bitcast_fusion.6
  216.6 0.3 fusion.90
  217.3 0.3 fusion.92
  220.1 2.2 convolution_convert_fusion.1
  222.4 0.5 all-gather.13.cloned.1.call-update
  223.0 26.1 %reduce-scatter.3.cloned.1.call-done = bf16[96,2048]{1,0:T(8,128)(2,1)} async-done(((bf16[384,2048]{1,0:T(8,128)(2,1)}), bf16[96,2048]{1,0:T(8,128)(2,1)}) %reduce-scatter.3.cloned.1.call-update) | async-done | bytes 393232 | tf_op jit(solution)/shard_map/reduce_scatter | solution.py:96
  249.1 1.2 multiply_reduce_fusion
  250.4 1.9 multiply_convert_fusion
  252.3 0.5 all-gather.15.cloned.1.call-update
  252.9 0.7 all-gather.17.cloned.1.call-update
  253.7 57.6 %all-gather.13.cloned.1.call-done = bf16[2048,768]{1,0:T(8,128)(2,1)} async-done(((bf16[256,768]{1,0:T(8,128)(2,1)}), bf16[2048,768]{1,0:T(8,128)(2,1)}) %all-gather.13.cloned.1.call-update) | async-done | bytes 3145744 | tf_op jit(solution)/shard_map/all_gather | solution.py:62
  311.2 19.7 %all-gather.11.cloned.1.call-done = bf16[384,2048]{1,0:T(8,128)(2,1)} async-done(((bf16[96,2048]{1,0:T(8,128)(2,1)}), bf16[384,2048]{1,0:T(8,128)(2,1)}) %all-gather.11.cloned.1.call-update) | async-done | bytes 1572880 | tf_op jit(solution)/shard_map/all_gather | solution.py:105
  331.0 4.8 fusion.55
  335.7 57.3 %all-gather.15.cloned.1.call-done = bf16[2048,768]{1,0:T(8,128)(2,1)} async-done(((bf16[256,768]{1,0:T(8,128)(2,1)}), bf16[2048,768]{1,0:T(8,128)(2,1)}) %all-gather.15.cloned.1.call-update) | async-done | bytes 3145744 | tf_op jit(solution)/shard_map/all_gather | solution.py:63
  393.0 63.4 %all-gather.17.cloned.1.call-done = bf16[768,2048]{1,0:T(8,128)(2,1)} async-done(((bf16[768,256]{1,0:T(8,128)(2,1)}), bf16[768,2048]{1,0:T(8,128)(2,1)}) %all-gather.17.cloned.1.call-update) | async-done | bytes 3145744 | tf_op jit(solution)/shard_map/all_gather | solution.py:111
  456.4 7.9 %convolution_convert_fusion = bf16[384,2048]{1,0:T(8,128)(2,1)} fusion(bf16[768,2048]{1,0:T(8,128)(2,1)} %all-gather.17.cloned.1.call-done, bf16[384,2048]{1,0:T(8,128)(2,1)} %all-gather.11.cloned.1.call-done, bf16[2048,768]{1,0:T(8,128)(2,1)} %all-gather.15.cloned.1.call-done, f32[384,768]{1,0:T(8,128)} %fusion.55), kind=kOutput, calls=%fused_computation.81 | convolution fusion | flops 2418475008 | bytes 10616832 | tf_op jit(solution)/shard_map/dot_general | solution.py:109
  464.3 26.4 %reduce-scatter.5.cloned.1.call-done = bf16[96,2048]{1,0:T(8,128)(2,1)} async-done(((bf16[384,2048]{1,0:T(8,128)(2,1)}), bf16[96,2048]{1,0:T(8,128)(2,1)}) %reduce-scatter.5.cloned.1.call-update) | async-done | bytes 393232 | tf_op jit(solution)/shard_map/reduce_scatter | solution.py:114
  490.7 1.9 add_convert_fusion
  (146 shorter events, 15.1 us)
Async XLA Ops:
  6.5 213.6 %copy-start = (bf16[512,2048]{1,0:T(8,128)(2,1)S(1)}, bf16[512,2048]{1,0:T(8,128)(2,1)}, u32[]{:S(2)}) copy-start(bf16[512,2048]{1,0:T(8,128)(2,1)} %param.17) | copy-start | bytes 6291460
  6.5 124.2 %all-gather.7.cloned.1.call-start = ((), (), s32[]{:S(2)}) async-start(), calls=%async_computation.2 | async-start | bytes 8847360 | tf_op jit(solution)/shard_map/all_gather | solution.py:72
  9.9 181.2 %all-gather.9.cloned.1.call-start = ((), (), s32[]{:S(2)}) async-start(), calls=%async_computation.3 | async-start | bytes 3538944 | tf_op jit(solution)/shard_map/all_gather | solution.py:78
  10.7 238.4 %reduce-scatter.3.cloned.1.call-start = ((), (), s32[]{:S(2)}) async-start(), calls=%async_computation.4 | async-start | bytes 1966080 | tf_op jit(solution)/shard_map/reduce_scatter | solution.py:96
  135.3 56.0 %copy-start.3 = (f32[384,4]{0,1:T(4,128)S(1)}, f32[384,4]{0,1:T(4,128)}, u32[]{:S(2)}) copy-start(f32[384,4]{0,1:T(4,128)} %param.15) | copy-start | bytes 18436
  135.3 56.0 %copy-start.5 = (bf16[384,512]{1,0:T(8,128)(2,1)S(1)}, bf16[384,512]{1,0:T(8,128)(2,1)}, u32[]{:S(2)}) copy-start(bf16[384,512]{1,0:T(8,128)(2,1)} %param.12) | copy-start | bytes 1179652
  222.3 0.7 copy-start.4
  222.3 26.8 %copy-start.1 = (bf16[96,2048]{1,0:T(8,128)(2,1)S(1)}, bf16[96,2048]{1,0:T(8,128)(2,1)}, u32[]{:S(2)}) copy-start(bf16[96,2048]{1,0:T(8,128)(2,1)} %param.16) | copy-start | bytes 1179652
  222.3 88.9 %all-gather.13.cloned.1.call-start = ((), (), s32[]{:S(2)}) async-start(), calls=%async_computation.6 | async-start | bytes 3538944 | tf_op jit(solution)/shard_map/all_gather | solution.py:62
  222.9 108.1 %all-gather.11.cloned.1.call-start = ((), (), s32[]{:S(2)}) async-start(), calls=%async_computation.5 | async-start | bytes 1966080 | tf_op jit(solution)/shard_map/all_gather | solution.py:105
  252.3 140.8 %all-gather.15.cloned.1.call-start = ((), (), s32[]{:S(2)}) async-start(), calls=%async_computation.7 | async-start | bytes 3538944 | tf_op jit(solution)/shard_map/all_gather | solution.py:63
  252.9 203.6 %all-gather.17.cloned.1.call-start = ((), (), s32[]{:S(2)}) async-start(), calls=%async_computation.8 | async-start | bytes 3538944 | tf_op jit(solution)/shard_map/all_gather | solution.py:111
  253.6 237.1 %reduce-scatter.5.cloned.1.call-start = ((), (), s32[]{:S(2)}) async-start(), calls=%async_computation.9 | async-start | bytes 1966080 | tf_op jit(solution)/shard_map/reduce_scatter | solution.py:114
  464.3 26.4 %copy-start.2 = (bf16[96,2048]{1,0:T(8,128)(2,1)S(1)}, bf16[96,2048]{1,0:T(8,128)(2,1)}, u32[]{:S(2)}) copy-start(bf16[96,2048]{1,0:T(8,128)(2,1)} %reduce-scatter.3.cloned.1.call-done) | copy-start | bytes 1179652
Sparse Core Ops, SparseCore 0:
  10.0 120.6 all-gather.6
  132.9 58.1 all-gather.8
  222.4 26.6 reduce-scatter.2
  251.2 60.0 all-gather.12
  312.6 18.2 all-gather.10
  333.0 60.0 all-gather.14
  395.1 61.2 all-gather.16
  464.4 26.2 reduce-scatter.4
